TPU v7x, 32 devices: a whole 2x2x4 slice. The times are simulated.
32 devices in a mesh: sp: 8 (over z, y), tp: 4 (over x, core).
Axes of the slice: x: 2, y: 2, z: 4, core: 2. Of those that a mesh axis runs over, the one named last changes fastest.
Arguments:
- latent: bfloat16 [1024, 2048], P(('sp', 'tp')), may hold values from -6 to 6
- context: bfloat16 [512, 2048], replicated, may hold values from -6 to 6
- condition: float32 [2048], replicated, may hold values from -6 to 6
- context_condition: float32 [2048], replicated, may hold values from -6 to 6
- modulation_weight: bfloat16 [2048, 3, 2048], P('sp', None, 'tp'), may hold values from -0.25 to 0.25
- norm_gain: float32 [2048], replicated, may hold values from 0.1 to 1.9
- gate_weight: bfloat16 [2048, 1024], P(None, 'tp'), may hold values from -0.125 to 0.125
- value_weight: bfloat16 [2048, 1024], P(None, 'tp'), may hold values from -0.125 to 0.125
- write_weight: bfloat16 [2048, 512], P(None, 'tp'), may hold values from -0.125 to 0.125
- read_weight: bfloat16 [2048, 512], P(None, 'tp'), may hold values from -0.125 to 0.125
- step_weight: bfloat16 [2048, 2, 16], replicated, may hold values from -0.125 to 0.125
- value_taps: bfloat16 [3, 1024], P(None, 'tp'), may hold values from -3.5 to 3.5
- map_taps: bfloat16 [3, 2, 512], P(None, None, 'tp'), may hold values from -3.5 to 3.5
- decay_rate: float32 [2, 16], replicated, may hold values from 1e-06 to 0.06
- decay_jump: float32 [2, 16, 1024], P(None, 'tp', 'sp'), may hold values from -2.76 to 0
- skip_gain: float32 [16], replicated, may hold values from 1 to 16
- group_gain: float32 [1024], P('tp'), may hold values from 0.1 to 1.9
- output_weight: bfloat16 [1024, 2048], P('tp'), may hold values from -0.1875 to 0.1875
- post_gain: float32 [2048], replicated, may hold values from 0.1 to 1.9
Outputs:
- updated: bfloat16 [1024, 2048], P(('sp', 'tp'))
All inputs are finite; a program needn't handle non-finite values.
Results may differ from a plain program's by a relative error of at most 0.014.
Values may be sent and summed in bfloat16 or wider, within the bound.
A program may use at most 64 MiB of HBM per device.

v0:
```python
import jax
import jax.numpy as jnp
from jax import lax
from jax.sharding import PartitionSpec as P

HEAD_DIM = 64
STATE = 64
SPAN = 128
EPSILON = 1e-06
HIGHEST = lax.Precision.HIGHEST


def carried_in_2(shard, axis, combine, identity, reverse):
    size, mine = (lax.axis_size(axis), lax.axis_index(axis))
    everything = jax.tree.map(
        lambda part, kind: lax.all_gather(part.astype(kind), axis),
        shard,
        jax.tree.map(lambda a: jnp.bfloat16 if a.dtype == jnp.float32 else a.dtype, shard),
    )
    start = jax.tree.map(
        lambda part, zero: jnp.broadcast_to(jnp.asarray(zero, part.dtype), part.shape),
        shard,
        identity,
    )

    def turn(k, before):
        at = size - 1 - k if reverse else k
        reached = at > mine if reverse else at < mine
        new = combine(
            before, jax.tree.map(lambda part, own: part[at].astype(own.dtype), everything, shard)
        )
        return jax.tree.map(lambda a, b: jnp.where(reached, a, b), new, before)

    return lax.fori_loop(0, size, turn, start)


def with_halo(cells, sides, width):
    for axis, dim in sides:
        count = lax.axis_size(axis)
        ends = count - 1
        head = lax.slice_in_dim(cells, 0, width, axis=dim)
        tail = lax.slice_in_dim(cells, cells.shape[dim] - width, cells.shape[dim], axis=dim)
        cells = jnp.concatenate(
            [
                lax.ppermute(tail, axis, [(i, (i + 1) % count) for i in range(ends)]),
                cells,
                lax.ppermute(head, axis, [((i + 1) % count, i) for i in range(ends)]),
            ],
            axis=dim,
        )
    return cells


def modulated_norm(row_block, gain_vec, shift_vec, scale_vec):
    widened = row_block.astype(jnp.float32)
    normed = widened * lax.rsqrt(jnp.mean(widened * widened, axis=-1, keepdims=True) + EPSILON)
    return (normed * gain_vec * (1.0 + scale_vec) + shift_vec).astype(jnp.bfloat16)


def short_conv(padded, conv_taps):
    length = padded.shape[0] - 2
    widened = padded.astype(jnp.float32)
    weights = conv_taps.astype(jnp.float32)
    summed = (
        weights[0] * widened[:length]
        + weights[1] * widened[1 : length + 1]
        + weights[2] * widened[2:]
    )
    return jax.nn.silu(summed)


def zero_rim(tensor):
    return jnp.pad(tensor, ((1, 1), (0, 0)))


def project(row_block, weight):
    return jnp.dot(row_block, weight, preferred_element_type=jnp.float32).astype(jnp.bfloat16)


def flip_rows(tensor, direction):
    if direction == 1:
        return jnp.flip(tensor, axis=0)
    return tensor


def sweep(inputs, step_sizes, log_decay, write_maps, read_maps, start_state):
    length, head_count, head_width = inputs.shape
    blocks = length // SPAN
    lower_mask = (jnp.arange(SPAN)[:, None] >= jnp.arange(SPAN)[None, :])[:, :, None]

    def cut_blocks(tensor):
        return tensor.reshape((blocks, SPAN) + tensor.shape[1:])

    def advance(carry_state, block_data):
        value_block, size_block, decay_block, write_block, read_block = block_data
        within = jnp.cumsum(decay_block, axis=0)
        weighted = value_block * size_block[:, :, None]
        log_gaps = jnp.where(lower_mask, within[:, None, :] - within[None, :, :], 0.0)
        fading = jnp.where(lower_mask, jnp.exp(log_gaps), 0.0)
        scores = jnp.einsum("ihn,jhn->ijh", read_block, write_block, precision=HIGHEST) * fading
        inner_term = jnp.einsum("ijh,jhp->ihp", scores, weighted, precision=HIGHEST)
        carried = jnp.einsum(
            "ihn,hpn->ihp", read_block * jnp.exp(within)[:, :, None], carry_state, precision=HIGHEST
        )
        block_total = within[-1]
        fresh_state = jnp.einsum(
            "jhn,jhp->hpn",
            write_block * jnp.exp(block_total[None, :] - within)[:, :, None],
            weighted,
            precision=HIGHEST,
        )
        return (
            jnp.exp(block_total)[:, None, None] * carry_state + fresh_state,
            inner_term + carried,
        )

    final_state, outputs = lax.scan(
        advance,
        start_state,
        (
            cut_blocks(inputs),
            cut_blocks(step_sizes),
            cut_blocks(log_decay),
            cut_blocks(write_maps),
            cut_blocks(read_maps),
        ),
    )
    return (outputs.reshape(length, head_count, head_width), final_state)


def chain_join(earlier, later):
    return (earlier[0] + later[0], jnp.exp(later[0])[:, None, None] * earlier[1] + later[1])


def carried_in(direction, element, identity):
    if direction == 0:
        return carried_in_2(element, "sp", chain_join, identity, False)
    return carried_in_2(element, "sp", chain_join, identity, True)


def body(
    latent,
    context,
    condition,
    context_condition,
    modulation_weight,
    norm_gain,
    gate_weight,
    value_weight,
    write_weight,
    read_weight,
    step_weight,
    value_taps,
    map_taps,
    decay_rate,
    decay_jump,
    skip_gain,
    group_gain,
    output_weight,
    post_gain,
):
    head_devices = lax.axis_size("tp")
    head_rank = lax.axis_index("tp")
    token_rank = lax.axis_index("sp")
    model_width = norm_gain.shape[0]
    own_rows = modulation_weight.shape[0]
    head_local = value_weight.shape[1] // HEAD_DIM
    group_local = write_weight.shape[1] // STATE
    conditions = jax.nn.silu(jnp.stack([condition, context_condition]))
    own_conditions = lax.dynamic_slice_in_dim(conditions, token_rank * own_rows, own_rows, 1)
    partial_value = jnp.einsum(
        "sd,dkc->skc", own_conditions, modulation_weight.astype(jnp.float32), precision=HIGHEST
    )
    column_share = partial_value.shape[2]
    placed = jnp.zeros((2, 3, head_devices, column_share), jnp.float32)
    placed = lax.dynamic_update_slice(placed, partial_value[:, :, None, :], (0, 0, head_rank, 0))
    modulation = lax.psum(placed, ("sp", "tp")).reshape(2, 3, model_width)
    head_start = head_rank * head_local
    rate_local = lax.dynamic_slice_in_dim(decay_rate, head_start, head_local, 1)
    skip_local = lax.dynamic_slice_in_dim(skip_gain, head_start, head_local, 0)
    own_step = lax.dynamic_slice_in_dim(step_weight, head_start, head_local, 2).reshape(
        model_width, 2 * head_local
    )
    normed = modulated_norm(latent, norm_gain, modulation[0, 0], modulation[0, 1])
    gathered = lax.all_gather(normed, "tp", axis=0, tiled=True)
    token_count = gathered.shape[0]
    gate_linear = project(gathered, gate_weight)
    step_linear = project(gathered, own_step).reshape(token_count, 2, head_local)
    joined = jnp.concatenate(
        [
            project(gathered, value_weight),
            project(gathered, write_weight),
            project(gathered, read_weight),
        ],
        axis=1,
    )
    padded = with_halo(joined, (("sp", 0),), 1)
    conv_taps = jnp.concatenate([value_taps, map_taps.reshape(3, -1)], axis=1)
    convolved = short_conv(padded, conv_taps)
    value_width = head_local * HEAD_DIM
    map_width = group_local * STATE
    repeat_count = head_local // group_local
    latent_values = convolved[:, :value_width].reshape(token_count, head_local, HEAD_DIM)
    latent_write = jnp.repeat(
        convolved[:, value_width : value_width + map_width].reshape(
            token_count, group_local, STATE
        ),
        repeat_count,
        axis=1,
    )
    latent_read = jnp.repeat(
        convolved[:, value_width + map_width :].reshape(token_count, group_local, STATE),
        repeat_count,
        axis=1,
    )
    normed_context = modulated_norm(context, norm_gain, modulation[1, 0], modulation[1, 1])
    context_value = project(normed_context, value_weight)
    context_map = project(normed_context, write_weight)
    context_step = project(normed_context, own_step)
    context_length = context_value.shape[0]
    context_values = short_conv(zero_rim(context_value), value_taps).reshape(
        context_length, head_local, HEAD_DIM
    )
    context_write = short_conv(zero_rim(context_map), map_taps[:, 0]).reshape(
        context_length, group_local, STATE
    )
    context_write = jnp.repeat(context_write, repeat_count, axis=1)
    context_step = context_step.reshape(context_length, 2, head_local)
    mixer_sum = skip_local[None, :, None] * latent_values
    identity = (
        jnp.zeros((head_local,), jnp.float32),
        jnp.zeros((head_local, HEAD_DIM, STATE), jnp.float32),
    )
    for direction in range(2):
        rate_head = rate_local[direction]
        latent_size = jax.nn.softplus(step_linear[:, direction].astype(jnp.float32))
        latent_decay = -latent_size * rate_head[None, :] + decay_jump[direction].T
        context_size = jax.nn.softplus(context_step[:, direction].astype(jnp.float32))
        context_decay = -context_size * rate_head[None, :]
        unused_rows, context_state = sweep(
            flip_rows(context_values, direction),
            flip_rows(context_size, direction),
            flip_rows(context_decay, direction),
            flip_rows(context_write, direction),
            flip_rows(context_write, direction),
            identity[1],
        )
        oriented_decay = flip_rows(latent_decay, direction)
        swept_rows, local_state = sweep(
            flip_rows(latent_values, direction),
            flip_rows(latent_size, direction),
            oriented_decay,
            flip_rows(latent_write, direction),
            flip_rows(latent_read, direction),
            identity[1],
        )
        cumulative = jnp.cumsum(oriented_decay, axis=0)
        before_log, before_state = carried_in(direction, (cumulative[-1], local_state), identity)
        entering = before_state + jnp.exp(before_log)[:, None, None] * context_state
        carried = jnp.einsum(
            "ihn,hpn->ihp",
            flip_rows(latent_read, direction) * jnp.exp(cumulative)[:, :, None],
            entering,
            precision=HIGHEST,
        )
        mixer_sum = mixer_sum + flip_rows(swept_rows + carried, direction)
    gated_rows = mixer_sum.reshape(token_count, value_width) * jax.nn.silu(
        gate_linear.astype(jnp.float32)
    )
    grouped = gated_rows.reshape(token_count, group_local, value_width // group_local)
    grouped = (
        grouped
        * lax.rsqrt(jnp.mean(grouped * grouped, axis=-1, keepdims=True) + EPSILON)
        * group_gain.reshape(group_local, value_width // group_local)
    )
    gated_rows = grouped.reshape(token_count, value_width).astype(jnp.bfloat16)
    mixed_rows = lax.psum_scatter(
        jnp.dot(gated_rows, output_weight, preferred_element_type=jnp.float32).astype(jnp.bfloat16),
        "tp",
        scatter_dimension=0,
        tiled=True,
    ).astype(jnp.float32)
    normed_out = (
        mixed_rows
        * lax.rsqrt(jnp.mean(mixed_rows * mixed_rows, axis=-1, keepdims=True) + EPSILON)
        * post_gain
    )
    return (latent.astype(jnp.float32) + modulation[0, 2] * normed_out).astype(jnp.bfloat16)


def solution(mesh):
    placed = (
        P(("sp", "tp"), None),
        P(),
        P(),
        P(),
        P("sp", None, "tp"),
        P(),
        P(None, "tp"),
        P(None, "tp"),
        P(None, "tp"),
        P(None, "tp"),
        P(),
        P(None, "tp"),
        P(None, None, "tp"),
        P(),
        P(None, "tp", "sp"),
        P(),
        P("tp"),
        P("tp", None),
        P(),
    )
    return jax.shard_map(
        body, mesh=mesh, in_specs=placed, out_specs=P(("sp", "tp"), None), check_vma=False
    )
```

profile of v0, /device:TPU:0, one launch (start us, length us, event | category | flops | bytes accessed | tf_op | source)
XLA Modules:
  0.0 261.5 jit_solution(11595066028982531883)
XLA Ops:
  6.5 1.8 convolution_bitcast_fusion.2
  8.5 42.4 %psum.7 = f32[2,3,2048]{2,0,1:T(2,128)S(1)} all-reduce(f32[2,3,2048]{2,0,1:T(2,128)S(1)} %reshape.310), channel_id=1, replica_groups=mesh['sp'=8,'tp'=4] {'sp','tp'}, use_global_device_ids=true, to_apply=%region_0.1 | all-reduce | flops 12288 | bytes 98304 | tf_op jit(solution)/shard_map/psum | solution.py:177
  53.7 7.9 %all_gather.23 = bf16[128,2048]{1,0:T(8,128)(2,1)S(1)} all-gather(bf16[32,2048]{1,0:T(8,128)(2,1)S(1)} %fusion.38), channel_id=1, replica_groups=mesh['sp'=8,'tp'=4] {'tp'}, dimensions={0}, use_global_device_ids=true | all-gather | bytes 655360 | tf_op jit(solution)/shard_map/all_gather | solution.py:185
  63.1 3.4 %collective-permute-start = (bf16[1,512]{1,0:T(2,128)(2,1)}, bf16[1,512]{1,0:T(2,128)(2,1)}, u32[]{:S(2)}, u32[]{:S(2)}) collective-permute-start(bf16[1,512]{1,0:T(2,128)(2,1)} %get-tuple-element.648), channel_id=1, source_target_pairs={{0,4},{4,8},{8,12},{12,16},{16,20},{20,24},{24,28},{1,5},{5,9},{9,... | collective-permute-start | bytes 3080 | tf_op jit(solution)/shard_map/ppermute | solution.py:45
  67.8 2.2 fusion.13
  70.9 1.4 convolution_convert_fusion.1
  72.3 1.4 convolution_convert_fusion.2
  74.7 2.2 convolution_convert_fusion.7
  88.5 7.4 %while.67 = (s32[]{:T(128)}, f32[4,64,64]{2,1,0:T(8,128)S(1)}, f32[4,128,4]{1,2,0:T(4,128)S(1)}, f32[4,128,4,64]{1,3,2,0:T(8,128)}, f32[4,128,4]{1,2,0:T(4,128)S...) while((s32[]{:T(128)}, f32[4,64,64]{2,1,0:T(8,128)S(1)}, ...), condition=%wide.region_8.9_spmd.clone, body=%wide.region_6.8_spmd.clone.sunk | while | flops 25346052 | bytes 684759 | solution.py:117
  97.8 1.6 rev.42
  99.4 3.4 %rev.41 = f32[512,4,64]{0,2,1:T(8,128)} reverse(f32[512,4,64]{0,2,1:T(8,128)} %bitcast.243), dimensions={0} | reverse | bytes 1048576 | tf_op jit(solution)/shard_map/jit(_flip)/rev | solution.py:82
  104.0 1.7 rev.43
  105.7 2.0 reshape.324
  107.7 8.1 %while.69 = (s32[]{:T(128)}, f32[4,64,64]{2,1,0:T(8,128)S(1)}, f32[4,128,4]{2,1,0:T(8,128)S(1)}, f32[4,128,4,64]{1,0,3,2:T(4,128)S(1)}, f32[4,128,4]{1,2,0:T(4,1...) while((s32[]{:T(128)}, f32[4,64,64]{2,1,0:T(8,128)S(1)}, ...), condition=%wide.region_14.15_spmd.clone, body=%wide.region_12.14_spmd.clone.sunk | while | flops 25346052 | bytes 942295 | solution.py:117
  108.0 1.3 constant_dynamic-slice_fusion.13
  110.1 1.3 constant_dynamic-slice_fusion.13
  112.1 1.3 constant_dynamic-slice_fusion.13
  116.6 20.7 %all-gather.2 = bf16[8,1,4]{2,1,0:T(2,128)(2,1)S(1)} all-gather(bf16[1,1,4]{2,1,0:T(2,128)(2,1)} %convert_bitcast_fusion.1), channel_id=1, replica_groups=mesh['sp'=8,'tp'=4] {'sp'}, dimensions={0}, use_global_device_ids=true | all-gather | bytes 72 | tf_op jit(solution)/shard_map/all_gather | solution.py:16
  137.2 16.4 %all-gather.3 = bf16[8,1,4]{2,1,0:T(2,128)(2,1)S(1)} all-gather(bf16[1,1,4]{2,1,0:T(2,128)(2,1)} %convert_bitcast_fusion), channel_id=1, replica_groups=mesh['sp'=8,'tp'=4] {'sp'}, dimensions={0}, use_global_device_ids=true | all-gather | bytes 72 | tf_op jit(solution)/shard_map/all_gather | solution.py:16
  159.2 31.2 %all-gather = bf16[32,64,64]{2,1,0:T(8,128)(2,1)S(1)} all-gather(bf16[4,64,64]{2,1,0:T(8,128)(2,1)S(1)} %fusion.26), channel_id=2, replica_groups=mesh['sp'=8,'tp'=4] {'sp'}, dimensions={0}, use_global_device_ids=true | all-gather | bytes 294912 | tf_op jit(solution)/shard_map/all_gather | solution.py:16
  192.0 31.7 %all-gather.1 = bf16[32,64,64]{2,1,0:T(8,128)(2,1)S(1)} all-gather(bf16[4,64,64]{2,1,0:T(8,128)(2,1)S(1)} %fusion.27), channel_id=3, replica_groups=mesh['sp'=8,'tp'=4] {'sp'}, dimensions={0}, use_global_device_ids=true | all-gather | bytes 294912 | tf_op jit(solution)/shard_map/all_gather | solution.py:16
  228.4 1.6 fusion.113
  231.6 20.2 %reduce-scatter.2.cloned.1.call-done = bf16[32,2048]{1,0:T(8,128)(2,1)} async-done(((bf16[128,2048]{1,0:T(8,128)(2,1)}), bf16[32,2048]{1,0:T(8,128)(2,1)}) %reduce-scatter.2.cloned.1.call-update) | async-done | bytes 131088 | tf_op jit(solution)/shard_map/reduce_scatter | solution.py:277
  252.9 1.7 fusion.39
  (282 shorter events, 49.7 us)
Async XLA Ops:
  6.5 223.9 %copy-start = (bf16[256,2048]{1,0:T(8,128)(2,1)S(1)}, bf16[256,2048]{1,0:T(8,128)(2,1)}, u32[]{:S(2)}) copy-start(bf16[256,2048]{1,0:T(8,128)(2,1)} %param.44) | copy-start | bytes 3145732
  6.5 55.0 %copy-start.5 = (bf16[2048,256]{1,0:T(8,128)(2,1)S(1)}, bf16[2048,256]{1,0:T(8,128)(2,1)}, u32[]{:S(2)}) copy-start(bf16[2048,256]{1,0:T(8,128)(2,1)} %param.34) | copy-start | bytes 3145732
  6.5 245.3 %reduce-scatter.2.cloned.1.call-start = ((), (), s32[]{:S(2)}) async-start(), calls=%async_computation.1 | async-start | bytes 655360 | tf_op jit(solution)/shard_map/reduce_scatter | solution.py:277
  8.3 53.9 %copy-start.3 = (bf16[2048,128]{1,0:T(8,128)(2,1)S(1)}, bf16[2048,128]{1,0:T(8,128)(2,1)}, u32[]{:S(2)}) copy-start(bf16[2048,128]{1,0:T(8,128)(2,1)} %param.35) | copy-start | bytes 1572868
  50.9 10.9 %copy-start.8 = (bf16[2048,128]{1,0:T(8,128)(2,1)S(1)}, bf16[2048,128]{1,0:T(8,128)(2,1)}, u32[]{:S(2)}) copy-start(bf16[2048,128]{1,0:T(8,128)(2,1)} %param.36) | copy-start | bytes 1572868
  61.9 8.1 %copy-start.16 = (f32[2048]{0:T(1024)S(1)}, f32[2048]{0:T(1024)}, u32[]{:S(2)}) copy-start(f32[2048]{0:T(1024)} %param.32) | copy-start | bytes 24580
  62.2 8.7 %copy-start.9 = (bf16[128,128]{1,0:T(8,128)(2,1)}, bf16[128,128]{1,0:T(8,128)(2,1)S(1)}, u32[]{:S(2)}) copy-start(bf16[128,128]{1,0:T(8,128)(2,1)S(1)} %convolution_convert_fusion.5) | copy-start | bytes 98308
  62.5 8.4 %copy-start.11 = (bf16[128,128]{1,0:T(8,128)(2,1)}, bf16[128,128]{1,0:T(8,128)(2,1)S(1)}, u32[]{:S(2)}) copy-start(bf16[128,128]{1,0:T(8,128)(2,1)S(1)} %convolution_convert_fusion.6) | copy-start | bytes 98308
  63.1 93.7 %collective-permute-start = (bf16[1,512]{1,0:T(2,128)(2,1)}, bf16[1,512]{1,0:T(2,128)(2,1)}, u32[]{:S(2)}, u32[]{:S(2)}) collective-permute-start(bf16[1,512]{1,0:T(2,128)(2,1)} %get-tuple-element.648), channel_id=1, source_target_pairs={{0,4},{4,8},{8,12},{12,16},{16,20},{20,24},{24,28},{1,5},{5,9},{9,... | collective-permute-start | bytes 3080 | tf_op jit(solution)/shard_map/ppermute | solution.py:45
  66.5 90.4 %collective-permute-start.1 = (bf16[1,512]{1,0:T(2,128)(2,1)}, bf16[1,512]{1,0:T(2,128)(2,1)}, u32[]{:S(2)}, u32[]{:S(2)}) collective-permute-start(bf16[1,512]{1,0:T(2,128)(2,1)} %get-tuple-element.649), channel_id=1, source_target_pairs={{4,0},{8,4},{12,8},{16,12},{20,16},{24,20},{28,24},{5,1},{9,5},{13... | collective-permute-start | bytes 3080 | tf_op jit(solution)/shard_map/ppermute | solution.py:47
  88.5 8.2 %copy-start.25 = (bf16[3,2,128]{2,1,0:T(2,128)(2,1)S(1)}, bf16[3,2,128]{2,1,0:T(2,128)(2,1)}, u32[]{:S(2)}) copy-start(bf16[3,2,128]{2,1,0:T(2,128)(2,1)} %param.39) | copy-start | bytes 4612
  88.5 8.2 %copy-start.22 = (bf16[3,256]{1,0:T(4,128)(2,1)S(1)}, bf16[3,256]{1,0:T(4,128)(2,1)}, u32[]{:S(2)}) copy-start(bf16[3,256]{1,0:T(4,128)(2,1)} %param.38) | copy-start | bytes 4612
  88.5 8.7 %copy-start.18 = (f32[512,4]{0,1:T(4,128)S(1)}, f32[512,4]{0,1:T(4,128)}, u32[]{:S(2)}) copy-start(f32[512,4]{0,1:T(4,128)} %get-tuple-element.662) | copy-start | bytes 24580
  107.7 47.2 %copy-start.14 = (f32[128,4]{1,0:T(8,128)S(1)}, f32[128,4]{1,0:T(8,128)}, u32[]{:S(2)}) copy-start(f32[128,4]{1,0:T(8,128)} %get-tuple-element.650) | copy-start | bytes 6148
  107.7 49.1 %copy-start.10 = (bf16[128,128]{1,0:T(8,128)(2,1)S(1)}, bf16[128,128]{1,0:T(8,128)(2,1)}, u32[]{:S(2)}) copy-start(bf16[128,128]{1,0:T(8,128)(2,1)} %copy-done.9) | copy-start | bytes 98308
  107.7 49.1 %copy-start.12 = (bf16[128,128]{1,0:T(8,128)(2,1)S(1)}, bf16[128,128]{1,0:T(8,128)(2,1)}, u32[]{:S(2)}) copy-start(bf16[128,128]{1,0:T(8,128)(2,1)} %copy-done.11) | copy-start | bytes 98308
  115.8 43.0 %copy-start.19 = (f32[128,4]{0,1:T(4,128)S(1)}, f32[128,4]{0,1:T(4,128)}, u32[]{:S(2)}) copy-start(f32[128,4]{0,1:T(4,128)} %get-tuple-element.668) | copy-start | bytes 6148
  115.9 43.0 %copy-start.30 = (f32[4]{0:T(128)S(1)}, f32[4]{0:T(128)}, u32[]{:S(2)}) copy-start(f32[4]{0:T(128)} %exponential_multiply_fusion.1) | copy-start | bytes 52
  155.0 35.5 %copy-start.20 = (f32[4]{0:T(128)S(1)}, f32[4]{0:T(128)}, u32[]{:S(2)}) copy-start(f32[4]{0:T(128)} %custom-call) | copy-start | bytes 52
  158.4 33.2 %copy-start.29 = (f32[4]{0:T(128)S(1)}, f32[4]{0:T(128)}, u32[]{:S(2)}) copy-start(f32[4]{0:T(128)} %exponential_multiply_fusion) | copy-start | bytes 52
  191.5 33.7 %copy-start.15 = (pred[128,128]{0,1:T(8,128)(4,1)S(1)}, pred[128,128]{0,1:T(8,128)(4,1)}, u32[]{:S(2)}) copy-start(pred[128,128]{0,1:T(8,128)(4,1)} %iota_compare_fusion) | copy-start | bytes 49156
  229.9 23.0 %copy-start.4 = (bf16[32,2048]{1,0:T(8,128)(2,1)S(1)}, bf16[32,2048]{1,0:T(8,128)(2,1)}, u32[]{:S(2)}) copy-start(bf16[32,2048]{1,0:T(8,128)(2,1)} %param.27) | copy-start | bytes 393220
  229.9 23.0 %copy-start.17 = (f32[1,1,2048]{2,0,1:T(1,128)S(1)}, f32[1,1,2048]{2,0,1:T(1,128)}, u32[]{:S(2)}) copy-start(f32[1,1,2048]{2,0,1:T(1,128)} %get-tuple-element.654) | copy-start | bytes 24580
  229.9 23.0 %copy-start.23 = (f32[2048]{0:T(1024)S(1)}, f32[2048]{0:T(1024)}, u32[]{:S(2)}) copy-start(f32[2048]{0:T(1024)} %param.45) | copy-start | bytes 24580
  (11 other events, 49.4 us)
Sparse Core Ops, SparseCore 0:
  231.8 20.0 reduce-scatter.1
where the time goes:
time: 263 us; the launch traced here: 261 us
  blocking collectives  150 us (57%)
  local copies, waits for them, and re-layouts  29.5 us (11%)
  other arithmetic  20.9 us (8%)
  matrix products  20.8 us (8%)
  waiting for transfers between devices  20.2 us (8%)
  between operations  14.2 us (5%)
  starting transfers between devices  4.64 us (2%)
    all_gather x4, blocking collectives, carried_in_2(): lax.all_gather(part.astype(kind), axis)  100 us
    psum x1, blocking collectives, body(): modulation = lax.psum(placed, ('sp', 'tp')).reshape(2, 3, model_width)  42.4 us
    reduce_scatter x1, waiting for transfers between devices, body(): lax.psum_scatter(jnp.dot(gated_rows, output_weight, preferred_element_typ...  20.2 us
    rev x12, local copies, waits for them, and re-layouts, flip_rows(): return jnp.flip(tensor, axis=0)  9.24 us
    all_gather x1, blocking collectives, body(): gathered = lax.all_gather(normed, 'tp', axis=0, tiled=True)  7.89 us
    dot_general x8, matrix products, project(): jnp.dot(row_block, weight, preferred_element_type=jnp.float32)  7.73 us
    dot_general x10, matrix products, advance(): jnp.einsum('jhn,jhp->hpn', write_block * jnp.exp(block_total[None, :] - w...  7.06 us
    dynamic_slice x16, local copies, waits for them, and re-layouts, sweep(): lax.scan(advance, start_state, (cut_blocks(inputs), cut_blocks(step_sizes...  6.44 us
  transfers between devices with their start and end apart: 3, of which 1 were waited for; matrix products, arithmetic and copies ran while one was open for 20% of the time, Pallas kernels for 0%

commit v1 on v0

--- a/solution.py
+++ b/solution.py
@@ -8,6 +8,11 @@
 SPAN = 128
 EPSILON = 1e-06
 HIGHEST = lax.Precision.HIGHEST
+
+
+def summed_here(value, name):
+    terms = lax.all_gather(value, name)
+    return jnp.sum(terms, axis=0)
 
 
 def carried_in_2(shard, axis, combine, identity, reverse):
@@ -174,7 +179,7 @@
     column_share = partial_value.shape[2]
     placed = jnp.zeros((2, 3, head_devices, column_share), jnp.float32)
     placed = lax.dynamic_update_slice(placed, partial_value[:, :, None, :], (0, 0, head_rank, 0))
-    modulation = lax.psum(placed, ("sp", "tp")).reshape(2, 3, model_width)
+    modulation = summed_here(placed, ("sp", "tp")).reshape(2, 3, model_width)
     head_start = head_rank * head_local
     rate_local = lax.dynamic_slice_in_dim(decay_rate, head_start, head_local, 1)
     skip_local = lax.dynamic_slice_in_dim(skip_gain, head_start, head_local, 0)

time: 263 us -> 298 us (1.13)
  waiting for transfers between devices: 20.2 us -> 65.8 us
  blocking collectives: 150 us -> 107 us
  other arithmetic: 20.9 us -> 40.7 us
  local copies, waits for them, and re-layouts: 29.5 us -> 40.6 us
    all_gather x0 -> x1, waiting for transfers between devices: none -> 46.1 us  [summed_here(): terms = lax.all_gather(value, name)]
    psum x1 -> x0, blocking collectives: 42.4 us -> none  [body(): modulation = lax.psum(placed, ('sp', 'tp')).reshape(2, 3, model_width)]
    exp x16, other arithmetic: 0.28 us -> 15.4 us  [chain_join(): jnp.exp(later[0])[:, None, None] * earlier[1] + later[1]]
    unnamed x70 -> x92, local copies, waits for them, and re-layouts: 2.66 us -> 5.74 us
  transfers between devices with their start and end apart: 3 -> 4, of which waited for: 1 -> 2; matrix products, arithmetic and copies ran while one was open for 20% -> 12% of each run, Pallas kernels for 0% -> 0%
where the time goes in v1:
time: 298 us; the launch traced here: 296 us
  blocking collectives  107 us (36%)
  waiting for transfers between devices  65.8 us (22%)
  other arithmetic  40.7 us (14%)
  local copies, waits for them, and re-layouts  40.6 us (14%)
  matrix products  22.1 us (7%)
  between operations  14.3 us (5%)
  starting transfers between devices  5.27 us (2%)
    all_gather x4, blocking collectives, carried_in_2(): lax.all_gather(part.astype(kind), axis)  99.3 us
    all_gather x1, waiting for transfers between devices, summed_here(): terms = lax.all_gather(value, name)  46.1 us
    reduce_scatter x1, waiting for transfers between devices, body(): lax.psum_scatter(jnp.dot(gated_rows, output_weight, preferred_element_typ...  19.7 us
    exp x16, other arithmetic, chain_join(): jnp.exp(later[0])[:, None, None] * earlier[1] + later[1]  15.4 us
    rev x12, local copies, waits for them, and re-layouts, flip_rows(): return jnp.flip(tensor, axis=0)  9.79 us
    dot_general x8, matrix products, project(): jnp.dot(row_block, weight, preferred_element_type=jnp.float32)  8.39 us
    dot_general x10, matrix products, advance(): jnp.einsum('jhn,jhp->hpn', write_block * jnp.exp(block_total[None, :] - w...  7.74 us
    all_gather x1, blocking collectives, body(): gathered = lax.all_gather(normed, 'tp', axis=0, tiled=True)  7.29 us
  transfers between devices with their start and end apart: 4, of which 2 were waited for; matrix products, arithmetic and copies ran while one was open for 12% of the time, Pallas kernels for 0%

profile of v1, /device:TPU:0, one launch (start us, length us, event | category | flops | bytes accessed | tf_op | source)
XLA Modules:
  0.0 296.4 jit_solution(13662566286590226844)
XLA Ops:
  6.5 1.7 convolution_bitcast_fusion.2
  19.0 2.1 fusion.13
  21.7 46.1 %all-gather.6.cloned.1.call-done = f32[32,2,3,4,512]{4,3,2,1,0:T(4,128)} async-done(((f32[1,2,3,4,512]{4,3,2,1,0:T(4,128)}), f32[32,2,3,4,512]{4,3,2,1,0:T(4,128)}) %all-gather.6.cloned.1.call-update) | async-done | bytes 1572880 | tf_op jit(solution)/shard_map/all_gather | solution.py:14
  67.8 2.3 reduce_sum.45
  71.5 1.5 reshape.313
  72.9 1.4 fusion.111
  76.5 1.4 convolution_convert_fusion.1
  78.0 7.3 %all_gather.31 = bf16[128,2048]{1,0:T(8,128)(2,1)S(1)} all-gather(bf16[32,2048]{1,0:T(8,128)(2,1)S(1)} %fusion.38), channel_id=1, replica_groups=mesh['sp'=8,'tp'=4] {'tp'}, dimensions={0}, use_global_device_ids=true | all-gather | bytes 655360 | tf_op jit(solution)/shard_map/all_gather | solution.py:190
  100.1 7.4 %while.67 = (s32[]{:T(128)}, f32[4,64,64]{2,1,0:T(8,128)S(1)}, f32[4,128,4]{1,2,0:T(4,128)S(1)}, f32[4,128,4,64]{1,3,2,0:T(8,128)}, f32[4,128,4]{1,2,0:T(4,128)S...) while((s32[]{:T(128)}, f32[4,64,64]{2,1,0:T(8,128)S(1)}, ...), condition=%wide.region_8.9_spmd.clone, body=%wide.region_6.8_spmd.clone.sunk | while | flops 25346052 | bytes 684759 | solution.py:122
  110.2 3.9 %collective-permute-start = (bf16[1,512]{1,0:T(2,128)(2,1)}, bf16[1,512]{1,0:T(2,128)(2,1)}, u32[]{:S(2)}, u32[]{:S(2)}) collective-permute-start(bf16[1,512]{1,0:T(2,128)(2,1)} %get-tuple-element.648), channel_id=1, source_target_pairs={{0,4},{4,8},{8,12},{12,16},{16,20},{20,24},{24,28},{1,5},{5,9},{9,... | collective-permute-start | bytes 3080 | tf_op jit(solution)/shard_map/ppermute | solution.py:50
  114.6 1.6 rev.42
  116.2 3.4 %rev.41 = f32[512,4,64]{0,2,1:T(8,128)} reverse(f32[512,4,64]{0,2,1:T(8,128)} %bitcast.243), dimensions={0} | reverse | bytes 1048576 | tf_op jit(solution)/shard_map/jit(_flip)/rev | solution.py:87
  120.8 1.7 rev.43
  122.5 2.0 reshape.327
  124.6 8.1 %while.69 = (s32[]{:T(128)}, f32[4,64,64]{2,1,0:T(8,128)S(1)}, f32[4,128,4]{2,1,0:T(8,128)S(1)}, f32[4,128,4,64]{1,0,3,2:T(4,128)S(1)}, f32[4,128,4]{1,2,0:T(4,1...) while((s32[]{:T(128)}, f32[4,64,64]{2,1,0:T(8,128)S(1)}, ...), condition=%wide.region_14.15_spmd.clone, body=%wide.region_12.14_spmd.clone.sunk | while | flops 25346052 | bytes 942295 | solution.py:122
  134.6 20.1 %all-gather.2 = bf16[8,1,4]{2,1,0:T(2,128)(2,1)S(1)} all-gather(bf16[1,1,4]{2,1,0:T(2,128)(2,1)} %convert_bitcast_fusion.1), channel_id=1, replica_groups=mesh['sp'=8,'tp'=4] {'sp'}, dimensions={0}, use_global_device_ids=true | all-gather | bytes 72 | tf_op jit(solution)/shard_map/all_gather | solution.py:21
  154.8 16.4 %all-gather.3 = bf16[8,1,4]{2,1,0:T(2,128)(2,1)S(1)} all-gather(bf16[1,1,4]{2,1,0:T(2,128)(2,1)} %convert_bitcast_fusion), channel_id=1, replica_groups=mesh['sp'=8,'tp'=4] {'sp'}, dimensions={0}, use_global_device_ids=true | all-gather | bytes 72 | tf_op jit(solution)/shard_map/all_gather | solution.py:21
  178.4 31.2 %all-gather = bf16[32,64,64]{2,1,0:T(8,128)(2,1)S(1)} all-gather(bf16[4,64,64]{2,1,0:T(8,128)(2,1)S(1)} %fusion.26), channel_id=2, replica_groups=mesh['sp'=8,'tp'=4] {'sp'}, dimensions={0}, use_global_device_ids=true | all-gather | bytes 294912 | tf_op jit(solution)/shard_map/all_gather | solution.py:21
  209.6 10.7 %while.66 = (s32[]{:T(128)}, f32[4]{0:T(128)}, f32[4,64,64]{2,1,0:T(8,128)S(1)}, s32[]{:T(128)}, bf16[8,4]{1,0:T(8,128)(2,1)}, /*index=5*/bf16[8,4,64,64]{3,2,1,0:T(8,128)(2,1)S(1)}, s32[]{:T(128)}, s32[]{:T(128)}) while((s32[]{:T(128)}, f32[4]{0:T(128)}, f32[4,64,64]{2,1,0:T(8,128)S(1)}, s32[]{:T(128)}, bf16[8,4]{1,0:T(8,128)(2,1)}, ...), condition=%wide.region_4.5_spmd.clone, body=%wide.region_3.4_spmd.clone.sunk | while | flops 81940 | bytes 164027 | solution.py:39
  222.1 31.6 %all-gather.1 = bf16[32,64,64]{2,1,0:T(8,128)(2,1)S(1)} all-gather(bf16[4,64,64]{2,1,0:T(8,128)(2,1)S(1)} %fusion.27), channel_id=3, replica_groups=mesh['sp'=8,'tp'=4] {'sp'}, dimensions={0}, use_global_device_ids=true | all-gather | bytes 294912 | tf_op jit(solution)/shard_map/all_gather | solution.py:21
  253.7 6.5 %while.68 = (s32[]{:T(128)}, f32[4]{0:T(128)S(1)}, f32[4,64,64]{2,1,0:T(8,128)S(1)}, s32[]{:T(128)}, bf16[8,4]{1,0:T(8,128)(2,1)}, /*index=5*/bf16[8,4,64,64]{3,...) while((s32[]{:T(128)}, f32[4]{0:T(128)S(1)}, f32[4,64,64]{2,1,0:T(8,128)S(1)}, ...), condition=%wide.region_11.12_spmd.clone, body=%wide.region_10.11_spmd.clone.sunk | while | flops 81944 | bytes 164089 | solution.py:39
  263.8 1.6 fusion.113
  267.1 19.7 %reduce-scatter.2.cloned.1.call-done = bf16[32,2048]{1,0:T(8,128)(2,1)} async-done(((bf16[128,2048]{1,0:T(8,128)(2,1)}), bf16[32,2048]{1,0:T(8,128)(2,1)}) %reduce-scatter.2.cloned.1.call-update) | async-done | bytes 131088 | tf_op jit(solution)/shard_map/reduce_scatter | solution.py:282
  287.8 1.7 fusion.39
  (308 shorter events, 82.5 us)
Async XLA Ops:
  6.5 259.4 %copy-start = (bf16[256,2048]{1,0:T(8,128)(2,1)S(1)}, bf16[256,2048]{1,0:T(8,128)(2,1)}, u32[]{:S(2)}) copy-start(bf16[256,2048]{1,0:T(8,128)(2,1)} %param.44) | copy-start | bytes 3145732
  6.5 14.6 %copy-start.30 = (bf16[3,256]{1,0:T(4,128)(2,1)S(1)}, bf16[3,256]{1,0:T(4,128)(2,1)}, u32[]{:S(2)}) copy-start(bf16[3,256]{1,0:T(4,128)(2,1)} %param.38) | copy-start | bytes 4612
  6.5 61.2 %all-gather.6.cloned.1.call-start = ((), (), s32[]{:S(2)}) async-start(), calls=%async_computation.1 | async-start | bytes 1622016 | tf_op jit(solution)/shard_map/all_gather | solution.py:14
  9.1 277.7 %reduce-scatter.2.cloned.1.call-start = ((), (), s32[]{:S(2)}) async-start(), calls=%async_computation.2 | async-start | bytes 655360 | tf_op jit(solution)/shard_map/reduce_scatter | solution.py:282
  11.4 63.0 %copy-start.1 = (bf16[512,2048]{1,0:T(8,128)(2,1)S(1)}, bf16[512,2048]{1,0:T(8,128)(2,1)}, u32[]{:S(2)}) copy-start(bf16[512,2048]{1,0:T(8,128)(2,1)} %param.28) | copy-start | bytes 6291460
  11.4 63.0 %copy-start.23 = (f32[2048]{0:T(1024)S(1)}, f32[2048]{0:T(1024)}, u32[]{:S(2)}) copy-start(f32[2048]{0:T(1024)} %param.32) | copy-start | bytes 24580
  100.0 9.5 %copy-start.7 = (bf16[128,256]{1,0:T(8,128)(2,1)S(1)}, bf16[128,256]{1,0:T(8,128)(2,1)}, u32[]{:S(2)}) copy-start(bf16[128,256]{1,0:T(8,128)(2,1)} %convolution_convert_fusion.4) | copy-start | bytes 196612
  100.0 9.5 %copy-start.15 = (bf16[128,128]{1,0:T(8,128)(2,1)S(1)}, bf16[128,128]{1,0:T(8,128)(2,1)}, u32[]{:S(2)}) copy-start(bf16[128,128]{1,0:T(8,128)(2,1)} %convolution_convert_fusion.6) | copy-start | bytes 98308
  100.1 14.1 %copy-start.25 = (f32[512,4]{0,1:T(4,128)S(1)}, f32[512,4]{0,1:T(4,128)}, u32[]{:S(2)}) copy-start(f32[512,4]{0,1:T(4,128)} %get-tuple-element.662) | copy-start | bytes 24580
  110.2 65.8 %collective-permute-start = (bf16[1,512]{1,0:T(2,128)(2,1)}, bf16[1,512]{1,0:T(2,128)(2,1)}, u32[]{:S(2)}, u32[]{:S(2)}) collective-permute-start(bf16[1,512]{1,0:T(2,128)(2,1)} %get-tuple-element.648), channel_id=1, source_target_pairs={{0,4},{4,8},{8,12},{12,16},{16,20},{20,24},{24,28},{1,5},{5,9},{9,... | collective-permute-start | bytes 3080 | tf_op jit(solution)/shard_map/ppermute | solution.py:50
  124.5 46.7 %copy-start.11 = (f32[128,4]{1,0:T(8,128)S(1)}, f32[128,4]{1,0:T(8,128)}, u32[]{:S(2)}) copy-start(f32[128,4]{1,0:T(8,128)} %copy-done.9) | copy-start | bytes 6148
  124.5 48.5 %copy-start.20 = (f32[128,4]{1,0:T(8,128)S(1)}, f32[128,4]{1,0:T(8,128)}, u32[]{:S(2)}) copy-start(f32[128,4]{1,0:T(8,128)} %get-tuple-element.650) | copy-start | bytes 6148
  124.5 51.4 %copy-start.8 = (bf16[128,256]{1,0:T(8,128)(2,1)S(1)}, bf16[128,256]{1,0:T(8,128)(2,1)}, u32[]{:S(2)}) copy-start(bf16[128,256]{1,0:T(8,128)(2,1)} %convolution_convert_fusion.4) | copy-start | bytes 196612
  124.5 51.4 %copy-start.16 = (bf16[128,128]{1,0:T(8,128)(2,1)S(1)}, bf16[128,128]{1,0:T(8,128)(2,1)}, u32[]{:S(2)}) copy-start(bf16[128,128]{1,0:T(8,128)(2,1)} %convolution_convert_fusion.6) | copy-start | bytes 98308
  124.6 51.4 %copy-start.18 = (bf16[128,128]{1,0:T(8,128)(2,1)S(1)}, bf16[128,128]{1,0:T(8,128)(2,1)}, u32[]{:S(2)}) copy-start(bf16[128,128]{1,0:T(8,128)(2,1)} %copy-done.17) | copy-start | bytes 98308
  132.7 45.3 %copy-start.26 = (f32[128,4]{0,1:T(4,128)S(1)}, f32[128,4]{0,1:T(4,128)}, u32[]{:S(2)}) copy-start(f32[128,4]{0,1:T(4,128)} %get-tuple-element.668) | copy-start | bytes 6148
  132.7 45.3 %copy-start.40 = (f32[4]{0:T(128)S(1)}, f32[4]{0:T(128)}, u32[]{:S(2)}) copy-start(f32[4]{0:T(128)} %exponential_multiply_fusion.1) | copy-start | bytes 52
  133.3 42.7 %collective-permute-start.1 = (bf16[1,512]{1,0:T(2,128)(2,1)}, bf16[1,512]{1,0:T(2,128)(2,1)S(1)}, u32[]{:S(2)}, u32[]{:S(2)}) collective-permute-start(bf16[1,512]{1,0:T(2,128)(2,1)} %get-tuple-element.649), channel_id=1, source_target_pairs={{4,0},{8,4},{12,8},{16,12},{20,16},{24,20},{28,24},{5,1},{9,5},{13... | collective-permute-start | bytes 3080 | tf_op jit(solution)/shard_map/ppermute | solution.py:52
  177.9 75.8 %copy-start.29 = (f32[4]{0:T(128)S(1)}, f32[4]{0:T(128)}, u32[]{:S(2)}) copy-start(f32[4]{0:T(128)} %custom-call.3) | copy-start | bytes 52
  220.3 40.3 %copy-start.22 = (pred[128,128]{0,1:T(8,128)(4,1)S(1)}, pred[128,128]{0,1:T(8,128)(4,1)}, u32[]{:S(2)}) copy-start(pred[128,128]{0,1:T(8,128)(4,1)} %iota_compare_fusion) | copy-start | bytes 49156
  222.1 39.5 %copy-start.28 = (f32[128,4]{0,1:T(4,128)S(1)}, f32[128,4]{0,1:T(4,128)}, u32[]{:S(2)}) copy-start(f32[128,4]{0,1:T(4,128)} %rev.36) | copy-start | bytes 6148
  265.4 22.4 %copy-start.5 = (bf16[32,2048]{1,0:T(8,128)(2,1)S(1)}, bf16[32,2048]{1,0:T(8,128)(2,1)}, u32[]{:S(2)}) copy-start(bf16[32,2048]{1,0:T(8,128)(2,1)} %param.27) | copy-start | bytes 393220
  265.4 22.4 %copy-start.24 = (f32[1,1,2048]{2,0,1:T(1,128)S(1)}, f32[1,1,2048]{2,0,1:T(1,128)}, u32[]{:S(2)}) copy-start(f32[1,1,2048]{2,0,1:T(1,128)} %get-tuple-element.654) | copy-start | bytes 24580
  265.4 22.4 %copy-start.31 = (f32[2048]{0:T(1024)S(1)}, f32[2048]{0:T(1024)}, u32[]{:S(2)}) copy-start(f32[2048]{0:T(1024)} %param.45) | copy-start | bytes 24580
  (23 other events, 95.4 us)
Sparse Core Ops, SparseCore 0:
  10.2 57.5 all-gather.5
  267.2 19.5 reduce-scatter.1
